TPU v7x, 32 devices: a whole 2x2x4 slice. The times are simulated.
32 devices in a mesh: sp: 8 (over z, x), dp: 4 (over y, core).
Axes of the slice: x: 2, y: 2, z: 4, core: 2. Of those that a mesh axis runs over, the one named last changes fastest.
Arguments:
- residual_in: bfloat16 [4, 1024, 2048], P('dp', 'sp'), may hold values from -6 to 6
- query_rows: bfloat16 [4, 1024, 1024], P('dp', 'sp'), may hold values from -40 to 40
- key_rows: bfloat16 [4, 1024, 1024], P('dp', 'sp'), may hold values from -40 to 40
- value_rows: bfloat16 [4, 1024, 1024], P('dp', 'sp'), may hold values from -6 to 6
- gate_sums: float32 [4, 16, 1024], P('dp', 'sp'), as said below
- out_weight: bfloat16 [1024, 2048], replicated, may hold values from -0.1875 to 0.1875
- mix_gain: float32 [2048], replicated, may hold values from 0.1 to 1.9
- ffn_gain: float32 [2048], replicated, may hold values from 0.1 to 1.9
- expert_ids: int32 [4, 1024, 4], P('dp', 'sp'), may hold values from 0 to 31, all different within a row; in each aligned block of 128 rows (0 to 127, 128 to 255, ..., all dimensions but the last counted through in order) at most 32 rows name the same one
- route_weights: float32 [4, 1024, 4], P('dp', 'sp'), may hold values from 0.3 to 2
- expert_gate: bfloat16 [32, 2048, 512], P(('sp', 'dp')), may hold values from -0.125 to 0.125
- expert_up: bfloat16 [32, 2048, 512], P(('sp', 'dp')), may hold values from -0.125 to 0.125
- expert_down: bfloat16 [32, 512, 2048], P(('sp', 'dp')), may hold values from -0.25 to 0.25
- shared_gate: bfloat16 [2048, 512], replicated, may hold values from -0.125 to 0.125
- shared_up: bfloat16 [2048, 512], replicated, may hold values from -0.125 to 0.125
- shared_down: bfloat16 [512, 2048], replicated, may hold values from -0.25 to 0.25
Outputs:
- result_rows: bfloat16 [4, 1024, 2048], P('dp', 'sp')
Inputs may be any that keep to these rules, and one draw needn't show every extreme that they name: `expert_ids`: each row names 4 different experts. In the rows of one device no expert is named more than 32 times, a bound that some block reaches in some devices' rows. `gate_sums`: Non-increasing along positions for every sequence and head.
All inputs are finite; a program needn't handle non-finite values.
Results may differ from a plain program's by a relative error of at most 0.0071.
Values may be sent and summed in bfloat16 or wider, within the bound.
A program may use at most 128 MiB of HBM per device.

v0:
```python
import jax
import jax.numpy as jnp
from jax import lax
from jax.sharding import PartitionSpec as P

HEAD_DIM = 64


def attend(query_all, key_all, value_all, gate_sums):
    length = query_all.shape[1]
    head_count = gate_sums.shape[1]
    score_scale = HEAD_DIM ** (-0.5)
    query_heads = query_all[0].reshape(length, head_count, HEAD_DIM)
    key_heads = key_all[0].reshape(length, head_count, HEAD_DIM)
    value_heads = value_all[0].reshape(length, head_count, HEAD_DIM)
    sums_local = gate_sums[0]
    block_rows = min(512, length)
    pieces = []
    for block_index in range(length // block_rows):
        start = block_index * block_rows
        block_end = start + block_rows
        scores = (
            jnp.einsum(
                "qhd,khd->hqk",
                query_heads[start:block_end],
                key_heads[:block_end],
                preferred_element_type=jnp.float32,
            )
            * score_scale
        )
        scores = scores + sums_local[:, start:block_end, None] - sums_local[:, None, :block_end]
        causal_mask = jnp.arange(block_end)[None, :] <= jnp.arange(start, block_end)[:, None]
        scores = jnp.where(causal_mask[None], scores, -jnp.inf)
        peak = jnp.max(scores, axis=2, keepdims=True)
        weights = jnp.exp(scores - peak)
        weights = (weights / jnp.sum(weights, axis=2, keepdims=True)).astype(jnp.bfloat16)
        mixed_heads = jnp.einsum(
            "hqk,khd->qhd", weights, value_heads[:block_end], preferred_element_type=jnp.float32
        ).astype(jnp.bfloat16)
        pieces.append(mixed_heads.reshape(block_rows, head_count * HEAD_DIM))
    return jnp.concatenate(pieces, axis=0)[None]


def gated_rows(rows_in, gate_w, up_w):
    gate_rows = jnp.dot(rows_in, gate_w, preferred_element_type=jnp.float32)
    up_rows = jnp.dot(rows_in, up_w, preferred_element_type=jnp.float32)
    return (jax.nn.silu(gate_rows) * up_rows).astype(jnp.bfloat16)


def shards(
    residual_in,
    query_rows,
    key_rows,
    value_rows,
    gate_sums,
    out_weight,
    mix_gain,
    ffn_gain,
    expert_ids,
    route_weights,
    expert_gate,
    expert_up,
    expert_down,
    shared_gate,
    shared_up,
    shared_down,
):
    query_all, key_all, value_all = (
        lax.all_to_all(query_rows, "sp", split_axis=2, concat_axis=1, tiled=True),
        lax.all_to_all(key_rows, "sp", split_axis=2, concat_axis=1, tiled=True),
        lax.all_to_all(value_rows, "sp", split_axis=2, concat_axis=1, tiled=True),
    )
    attended = attend(query_all, key_all, value_all, gate_sums)
    returned = lax.all_to_all(attended, "sp", split_axis=1, concat_axis=2, tiled=True)
    projected = jnp.dot(returned[0], out_weight, preferred_element_type=jnp.float32)
    residual_f = residual_in[0].astype(jnp.float32)
    mixed_rows = residual_f + mix_gain * projected * lax.rsqrt(
        jnp.mean(projected * projected, axis=1, keepdims=True) + 1e-06
    )
    normed = (
        ffn_gain
        * mixed_rows
        * lax.rsqrt(jnp.mean(mixed_rows * mixed_rows, axis=1, keepdims=True) + 1e-06)
    ).astype(jnp.bfloat16)
    shared_hidden = gated_rows(normed, shared_gate, shared_up)
    shared_out = jnp.dot(shared_hidden, shared_down, preferred_element_type=jnp.float32)
    tok_count = residual_in.shape[1]
    top_count = expert_ids.shape[2]
    width = residual_in.shape[2]
    sp_count = lax.axis_size("sp")
    dp_count = lax.axis_size("dp")
    expert_count = sp_count * dp_count
    capacity = 2 * tok_count * top_count // expert_count
    expert_list = expert_ids[0].reshape(tok_count * top_count)
    one_hot = (expert_list[:, None] == jnp.arange(expert_count, dtype=jnp.int32)[None, :]).astype(
        jnp.int32
    )
    position_in = jnp.sum((jnp.cumsum(one_hot, axis=0) - one_hot) * one_hot, axis=1)
    slot_index = expert_list * capacity + position_in
    repeated = jnp.repeat(normed, top_count, axis=0)
    outgoing = (
        jnp.zeros((expert_count * capacity, width), jnp.bfloat16).at[slot_index].set(repeated)
    )
    arrived = lax.all_to_all(
        outgoing.reshape(expert_count, capacity, width),
        ("sp", "dp"),
        split_axis=0,
        concat_axis=0,
        tiled=True,
    )
    flat_rows = arrived.reshape(-1, width)
    hidden = gated_rows(flat_rows, expert_gate[0], expert_up[0])
    finished = jnp.dot(hidden, expert_down[0], preferred_element_type=jnp.float32).astype(
        jnp.bfloat16
    )
    received = lax.all_to_all(
        finished.reshape(arrived.shape), ("sp", "dp"), split_axis=0, concat_axis=0, tiled=True
    )
    picked = received.reshape(expert_count * capacity, width)[slot_index]
    picked = picked.reshape(tok_count, top_count, width).astype(jnp.float32)
    routed = jnp.sum(picked * route_weights[0][:, :, None], axis=1)
    result_rows = (mixed_rows + shared_out + routed).astype(jnp.bfloat16)
    return result_rows[None]


def solution(mesh):
    return jax.shard_map(
        shards,
        mesh=mesh,
        in_specs=(
            P("dp", "sp", None),
            P("dp", "sp", None),
            P("dp", "sp", None),
            P("dp", "sp", None),
            P("dp", "sp", None),
            P(),
            P(),
            P(),
            P("dp", "sp", None),
            P("dp", "sp", None),
            P(("sp", "dp"), None, None),
            P(("sp", "dp"), None, None),
            P(("sp", "dp"), None, None),
            P(),
            P(),
            P(),
        ),
        out_specs=P("dp", "sp", None),
        check_vma=False,
    )
```

profile of v0, /device:TPU:0, one launch (start us, length us, event | category | flops | bytes accessed | tf_op | source)
XLA Modules:
  0.0 328.5 jit_solution(7871897657675203846)
XLA Ops:
  0.0 1.4 copy.60
  1.4 0.5 broadcast.123
  2.0 2.2 reduce.4
  4.2 0.8 reshape.174
  4.9 7.3 %all-to-all-start.1 = ((bf16[8,2,8192]{2,1,0:T(2,128)(2,1)}), bf16[8,2,8192]{2,1,0:T(2,128)(2,1)S(1)}, u32[]{:S(2)}, u32[]{:S(2)}) async-start(bf16[8,2,8192]{2,1,0:T(2,128)(2,1)} %reshape.174), calls=%async_computation.1 | async-start | bytes 524288 | tf_op jit(solution)/shard_map/all_to_all | solution.py:70
  13.0 2.2 reduce.3
  15.2 0.8 reshape.172
  16.3 2.2 reduce.2
  18.5 0.8 reshape.170
  19.3 1.8 all-to-all-done.1
  21.1 4.2 %all-to-all-start.2 = ((bf16[8,2,8192]{2,1,0:T(2,128)(2,1)}), bf16[8,2,8192]{2,1,0:T(2,128)(2,1)S(1)}, u32[]{:S(2)}, u32[]{:S(2)}) async-start(bf16[8,2,8192]{2,1,0:T(2,128)(2,1)} %reshape.170), calls=%async_computation.2 | async-start | bytes 524288 | tf_op jit(solution)/shard_map/all_to_all | solution.py:71
  25.3 1.2 reduce-window.6
  26.7 0.8 iota_compare_fusion.1
  27.5 6.3 %all-to-all-done.2 = bf16[8,2,8192]{2,1,0:T(2,128)(2,1)S(1)} async-done(((bf16[8,2,8192]{2,1,0:T(2,128)(2,1)}), bf16[8,2,8192]{2,1,0:T(2,128)(2,1)S(1)}, u32[]{:S(2)}, u32[]{:S(2)}) %all-to-all-start.2) | async-done | bytes 262176 | tf_op jit(solution)/shard_map/all_to_all | solution.py:71
  33.8 3.6 %all-to-all-start = ((bf16[8,2,8192]{2,1,0:T(2,128)(2,1)}), bf16[8,2,8192]{2,1,0:T(2,128)(2,1)S(1)}, u32[]{:S(2)}, u32[]{:S(2)}) async-start(bf16[8,2,8192]{2,1,0:T(2,128)(2,1)} %reshape.172), calls=%async_computation | async-start | bytes 524288 | tf_op jit(solution)/shard_map/all_to_all | solution.py:69
  37.5 1.2 iota_compare_fusion
  39.1 0.7 slice.53
  40.3 0.7 slice.51
  40.9 5.0 %all-to-all-done = bf16[8,2,8192]{2,1,0:T(2,128)(2,1)S(1)} async-done(((bf16[8,2,8192]{2,1,0:T(2,128)(2,1)}), bf16[8,2,8192]{2,1,0:T(2,128)(2,1)S(1)}, u32[]{:S(2)}, u32[]{:S(2)}) %all-to-all-start) | async-done | bytes 262176 | tf_op jit(solution)/shard_map/all_to_all | solution.py:69
  46.4 0.7 slice.45
  47.1 0.8 reshape_squeeze.8
  47.9 0.8 reshape_squeeze.9
  48.7 2.9 fusion.54
  51.7 3.9 %fusion.22 = bf16[2,512,64]{1,2,0:T(8,128)(2,1)S(1)} fusion(bf16[1024,2,64]{0,2,1:T(8,128)(2,1)} %reshape_squeeze.9, f32[2,512]{1,0:T(2,128)S(1)} %fusion.54, f32[2,1024]{1,0:T(2,128)S(1)} %bitcast.143, f32[2,512]{1,0:T(2,128)S(1)} %get-tuple-element.8, pred[512,1024]{1,0:T(8,128)(4,1)S(1)} %copy-done.4, bf16[512,2,64]{0,2,1:T(8,128)(2,1)} %slice.45, ...), kind=kOutput, calls=%fused_computation.35 | convolution fusion | flops 275843072 | bytes 1327104 | tf_op jit(solution)/shard_map/hqk,khd->qhd/dot_general | solution.py:37
  56.2 1.1 fusion.55
  57.3 1.3 convolution_convert_fusion.1
  58.8 0.4 copy.85
  59.2 2.2 reduce.5
  61.4 0.8 reshape.176
  62.2 3.8 %all-to-all-start.3 = ((bf16[8,2,8192]{2,1,0:T(2,128)(2,1)}), bf16[8,2,8192]{2,1,0:T(2,128)(2,1)S(1)}, u32[]{:S(2)}, u32[]{:S(2)}) async-start(bf16[8,2,8192]{2,1,0:T(2,128)(2,1)} %reshape.176), calls=%async_computation.3 | async-start | bytes 524288 | tf_op jit(solution)/shard_map/all_to_all | solution.py:74
  66.3 8.1 %all-to-all-done.3 = bf16[8,2,8192]{2,1,0:T(2,128)(2,1)S(1)} async-done(((bf16[8,2,8192]{2,1,0:T(2,128)(2,1)}), bf16[8,2,8192]{2,1,0:T(2,128)(2,1)S(1)}, u32[]{:S(2)}, u32[]{:S(2)}) %all-to-all-start.3) | async-done | bytes 262176 | tf_op jit(solution)/shard_map/all_to_all | solution.py:74
  75.0 3.1 multiply_reduce_fusion.2
  78.4 0.4 multiply_convert_fusion.1
  78.9 0.8 copy-done.1
  79.7 2.4 broadcast_in_dim.38
  82.1 4.0 %reshape.163 = bf16[512,2048]{1,0:T(8,128)(2,1)} reshape(bf16[128,4,2048]{2,1,0:T(4,128)(2,1)} %broadcast_in_dim.38) | data formatting | bytes 4194304 | tf_op jit(solution)/shard_map/reshape | solution.py:100
  86.1 7.2 %scatter_custom_fusion = bf16[1024,2048]{1,0:T(8,128)(2,1)} fusion(s32[512]{0:T(512)S(1)} %bitcast.138, bf16[512,2048]{1,0:T(8,128)(2,1)} %reshape.163, bf16[]{:T(256)} %constant.10.clone.1), kind=kCustom, calls=%fused_computation.20 | custom fusion | bytes 4194816 | tf_op jit(solution)/shard_map/scatter | solution.py:102
  93.3 97.2 %all_to_all.70 = bf16[32,32,2048]{2,1,0:T(8,128)(2,1)S(1)} all-to-all(bf16[32,32,2048]{2,1,0:T(8,128)(2,1)} %bitcast.117), channel_id=1, replica_groups=mesh['sp'=8,'dp'=4] {'sp','dp'}, dimensions={0} | all-to-all | bytes 8388608 | tf_op jit(solution)/shard_map/all_to_all | solution.py:104
  190.5 2.0 copy-done.3
  192.5 3.7 %fusion.7 = f32[1024,512]{1,0:T(8,128)} fusion(bf16[1024,2048]{1,0:T(8,128)(2,1)S(1)} %bitcast.119, bf16[1,2048,512]{2,1,0:T(8,128)(2,1)S(1)} %copy-done.16), kind=kOutput, calls=%fused_computation.15 | convolution fusion | flops 2147483648 | bytes 8388608 | tf_op jit(solution)/shard_map/dot_general | solution.py:46
  196.2 10.1 %convolution_convert_fusion = bf16[1024,2048]{1,0:T(8,128)(2,1)} fusion(bf16[1,512,2048]{2,1,0:T(8,128)(2,1)S(1)} %copy-done, f32[1024,512]{1,0:T(8,128)} %fusion.7, bf16[1024,2048]{1,0:T(8,128)(2,1)} %bitcast.120, bf16[1,2048,512]{2,1,0:T(8,128)(2,1)} %param.26), kind=kOutput, calls=%fused_computation.8 | convolution fusion | flops 4300210176 | bytes 14680064 | tf_op jit(solution)/shard_map/dot_general | solution.py:113
  206.2 4.0 %all-to-all-start.5 = ((bf16[32,32,2048]{2,1,0:T(8,128)(2,1)}), bf16[32,32,2048]{2,1,0:T(8,128)(2,1)}, u32[]{:S(2)}, u32[]{:S(2)}) async-start(bf16[32,32,2048]{2,1,0:T(8,128)(2,1)} %bitcast.118), calls=%async_computation.5 | async-start | bytes 8388608 | tf_op jit(solution)/shard_map/all_to_all | solution.py:116
  210.4 2.2 fusion.56
  212.7 91.9 %all-to-all-done.5 = bf16[32,32,2048]{2,1,0:T(8,128)(2,1)} async-done(((bf16[32,32,2048]{2,1,0:T(8,128)(2,1)}), bf16[32,32,2048]{2,1,0:T(8,128)(2,1)}, u32[]{:S(2)}, u32[]{:S(2)}) %all-to-all-start.5) | async-done | bytes 4194336 | tf_op jit(solution)/shard_map/all_to_all | solution.py:116
  304.5 8.0 %gather_fusion = bf16[512,2048]{1,0:T(8,128)(2,1)} fusion(bf16[1024,2048]{1,0:T(8,128)(2,1)} %bitcast.21, s32[1024]{0:T(1024)S(1)} %pad_clamp_fusion), kind=kCustom, calls=%fused_computation | custom fusion | bytes 4196352 | tf_op jit(solution)/shard_map/gather | solution.py:119
  312.5 4.8 %reshape.150 = f32[128,4,2048]{2,1,0:T(4,128)} reshape(bf16[512,2048]{1,0:T(8,128)(2,1)} %gather_fusion) | data formatting | bytes 6291456 | tf_op jit(solution)/shard_map/convert_element_type | solution.py:120
  317.2 6.3 %multiply_reduce_fusion = f32[128,2048]{1,0:T(8,128)} fusion(f32[128,4,2048]{2,1,0:T(4,128)} %reshape.150, f32[128,4]{1,0:T(8,128)S(1)} %copy.76), kind=kLoop, calls=%fused_computation.4 | loop fusion | flops 1835008 | bytes 5244928 | tf_op jit(solution)/shard_map/reduce_sum | solution.py:121
  323.6 4.5 %fusion.5 = bf16[1,128,2048]{2,1,0:T(8,128)(2,1)} fusion(f32[128,2048]{1,0:T(8,128)} %multiply_reduce_fusion, bf16[512,2048]{1,0:T(8,128)(2,1)} %param.31, bf16[128,2048]{1,0:T(8,128)(2,1)} %copy-done.1, bf16[2048,512]{1,0:T(8,128)(2,1)} %param.30, f32[128,512]{1,0:T(8,128)S(1)} %fusion.56, f32[128]{0:T(128)S(1)} %add_rsqrt_fusion.1, ...), kind=kOutput, calls=%fused_computation.13 | convolution fusion | flops 539099136 | bytes 8135168 | tf_op jit(solution)/shard_map/dot_general | solution.py:86
  (76 shorter events, 4.9 us)
Async XLA Ops:
  0.0 196.2 %copy-start = (bf16[1,512,2048]{2,1,0:T(8,128)(2,1)S(1)}, bf16[1,512,2048]{2,1,0:T(8,128)(2,1)}, u32[]{:S(2)}) copy-start(bf16[1,512,2048]{2,1,0:T(8,128)(2,1)} %param.28) | copy-start | bytes 6291460
  0.0 12.2 %copy-start.13 = (s32[1,128,4]{1,2,0:T(4,128)S(1)}, s32[1,128,4]{1,2,0:T(4,128)}, u32[]{:S(2)}) copy-start(s32[1,128,4]{1,2,0:T(4,128)} %param.24) | copy-start | bytes 6148
  0.0 12.5 %copy-start.7 = (bf16[1,128,1024]{2,1,0:T(8,128)(2,1)S(1)}, bf16[1,128,1024]{2,1,0:T(8,128)(2,1)}, u32[]{:S(2)}) copy-start(bf16[1,128,1024]{2,1,0:T(8,128)(2,1)} %param.17) | copy-start | bytes 786436
  1.4 14.5 %copy-start.8 = (bf16[1,128,1024]{2,1,0:T(8,128)(2,1)S(1)}, bf16[1,128,1024]{2,1,0:T(8,128)(2,1)}, u32[]{:S(2)}) copy-start(bf16[1,128,1024]{2,1,0:T(8,128)(2,1)} %param.19) | copy-start | bytes 786436
  4.9 16.2 %all-to-all-start.1 = ((bf16[8,2,8192]{2,1,0:T(2,128)(2,1)}), bf16[8,2,8192]{2,1,0:T(2,128)(2,1)S(1)}, u32[]{:S(2)}, u32[]{:S(2)}) async-start(bf16[8,2,8192]{2,1,0:T(2,128)(2,1)} %reshape.174), calls=%async_computation.1 | async-start | bytes 524288 | tf_op jit(solution)/shard_map/all_to_all | solution.py:70
  15.1 22.3 %copy-start.14 = (f32[1,2,1024]{2,1,0:T(2,128)S(1)}, f32[1,2,1024]{2,1,0:T(2,128)}, u32[]{:S(2)}) copy-start(f32[1,2,1024]{2,1,0:T(2,128)} %param.20) | copy-start | bytes 24580
  21.1 12.7 %all-to-all-start.2 = ((bf16[8,2,8192]{2,1,0:T(2,128)(2,1)}), bf16[8,2,8192]{2,1,0:T(2,128)(2,1)S(1)}, u32[]{:S(2)}, u32[]{:S(2)}) async-start(bf16[8,2,8192]{2,1,0:T(2,128)(2,1)} %reshape.170), calls=%async_computation.2 | async-start | bytes 524288 | tf_op jit(solution)/shard_map/all_to_all | solution.py:71
  26.7 13.3 %copy-start.11 = (s32[32,5]{0,1:T(8,128)}, s32[32,5]{0,1:T(8,128)S(1)}, u32[]{:S(2)}) copy-start(s32[32,5]{0,1:T(8,128)S(1)} %reduce-window.9) | copy-start | bytes 1924
  33.8 12.1 %all-to-all-start = ((bf16[8,2,8192]{2,1,0:T(2,128)(2,1)}), bf16[8,2,8192]{2,1,0:T(2,128)(2,1)S(1)}, u32[]{:S(2)}, u32[]{:S(2)}) async-start(bf16[8,2,8192]{2,1,0:T(2,128)(2,1)} %reshape.172), calls=%async_computation | async-start | bytes 524288 | tf_op jit(solution)/shard_map/all_to_all | solution.py:69
  46.2 2.5 copy-start.4
  51.7 4.2 %copy-start.5 = (bf16[1,4,128,128]{2,3,1,0:T(8,128)(2,1)S(1)}, bf16[1,4,128,128]{2,3,1,0:T(8,128)(2,1)}, u32[]{:S(2)}) copy-start(bf16[1,4,128,128]{2,3,1,0:T(8,128)(2,1)} %slice.53) | copy-start | bytes 393220
  51.7 4.4 %copy-start.6 = (bf16[1,4,128,128]{2,3,1,0:T(8,128)(2,1)S(1)}, bf16[1,4,128,128]{2,3,1,0:T(8,128)(2,1)}, u32[]{:S(2)}) copy-start(bf16[1,4,128,128]{2,3,1,0:T(8,128)(2,1)} %slice.51) | copy-start | bytes 393220
  51.7 4.6 %copy-start.9 = (pred[512,512]{0,1:T(8,128)(4,1)S(1)}, pred[512,512]{0,1:T(8,128)(4,1)}, u32[]{:S(2)}) copy-start(pred[512,512]{0,1:T(8,128)(4,1)} %iota_compare_fusion.1) | copy-start | bytes 786436
  58.6 7.6 %slice-start = ((s32[32,5]{0,1:T(8,128)}), s32[32,4]{0,1:T(4,128)S(1)}, s32[]{:S(2)}) async-start(s32[32,5]{0,1:T(8,128)} %copy-done.11), calls=%async_computation.6 | async-start | bytes 4096 | tf_op jit(solution)/shard_map/slice.1
  62.2 12.3 %all-to-all-start.3 = ((bf16[8,2,8192]{2,1,0:T(2,128)(2,1)}), bf16[8,2,8192]{2,1,0:T(2,128)(2,1)S(1)}, u32[]{:S(2)}, u32[]{:S(2)}) async-start(bf16[8,2,8192]{2,1,0:T(2,128)(2,1)} %reshape.176), calls=%async_computation.3 | async-start | bytes 524288 | tf_op jit(solution)/shard_map/all_to_all | solution.py:74
  74.9 3.1 copy-start.2
  75.0 3.1 copy-start.10
  75.0 3.5 %copy-start.12 = (f32[2048]{0:T(1024)S(1)}, f32[2048]{0:T(1024)}, u32[]{:S(2)}) copy-start(f32[2048]{0:T(1024)} %param.23) | copy-start | bytes 24580
  78.9 0.8 copy-start.1
  93.3 99.2 %copy-start.16 = (bf16[1,2048,512]{2,1,0:T(8,128)(2,1)S(1)}, bf16[1,2048,512]{2,1,0:T(8,128)(2,1)}, u32[]{:S(2)}) copy-start(bf16[1,2048,512]{2,1,0:T(8,128)(2,1)} %param.27) | copy-start | bytes 6291460
  190.5 2.0 copy-start.3
  206.2 4.1 %copy-start.15 = (f32[1,128,4]{1,2,0:T(4,128)S(1)}, f32[1,128,4]{1,2,0:T(4,128)}, u32[]{:S(2)}) copy-start(f32[1,128,4]{1,2,0:T(4,128)} %param.25) | copy-start | bytes 6148
  206.2 98.3 %all-to-all-start.5 = ((bf16[32,32,2048]{2,1,0:T(8,128)(2,1)}), bf16[32,32,2048]{2,1,0:T(8,128)(2,1)}, u32[]{:S(2)}, u32[]{:S(2)}) async-start(bf16[32,32,2048]{2,1,0:T(8,128)(2,1)} %bitcast.118), calls=%async_computation.5 | async-start | bytes 8388608 | tf_op jit(solution)/shard_map/all_to_all | solution.py:116
where the time goes:
time: 335 us; the launch traced here: 329 us
  waiting for transfers between devices  113 us (34%)
  blocking collectives  97.2 us (29%)
  local copies, waits for them, and re-layouts  42.5 us (13%)
  matrix products  32.8 us (10%)
  starting transfers between devices  22.9 us (7%)
  other arithmetic  19.1 us (6%)
    all_to_all x1, blocking collectives, shards(): lax.all_to_all(outgoing.reshape(expert_count, capacity, width), ('sp', 'd...  97.2 us
    all_to_all x1, waiting for transfers between devices, shards(): lax.all_to_all(finished.reshape(arrived.shape), ('sp', 'dp'), split_axis=...  91.9 us
    dot_general x1, matrix products, shards(): jnp.dot(hidden, expert_down[0], preferred_element_type=jnp.float32)  10.1 us
    unnamed x51, local copies, waits for them, and re-layouts  9.95 us
    unnamed x4, other arithmetic  8.73 us
    all_to_all x1, waiting for transfers between devices, shards(): lax.all_to_all(attended, 'sp', split_axis=1, concat_axis=2, tiled=True)  8.12 us
    gather x1, local copies, waits for them, and re-layouts, shards(): picked = received.reshape(expert_count * capacity, width)[slot_index]  7.96 us
    all_to_all x1, starting transfers between devices, shards(): lax.all_to_all(key_rows, 'sp', split_axis=2, concat_axis=1, tiled=True)  7.29 us
  transfers between devices with their start and end apart: 5, of which 5 were waited for; matrix products, arithmetic and copies ran while one was open for 5% of the time, Pallas kernels for 0%

commit v1 on v0

--- a/solution.py
+++ b/solution.py
@@ -1,6 +1,11 @@
+import functools
+import math
+
 import jax
 import jax.numpy as jnp
 from jax import lax
+from jax.experimental import pallas as pl
+from jax.experimental.pallas import tpu as pltpu
 from jax.sharding import PartitionSpec as P
 
 HEAD_DIM = 64
@@ -91,36 +96,281 @@
     dp_count = lax.axis_size("dp")
     expert_count = sp_count * dp_count
     capacity = 2 * tok_count * top_count // expert_count
+    groups = math.gcd(sp_count, top_count)
     expert_list = expert_ids[0].reshape(tok_count * top_count)
     one_hot = (expert_list[:, None] == jnp.arange(expert_count, dtype=jnp.int32)[None, :]).astype(
         jnp.int32
     )
     position_in = jnp.sum((jnp.cumsum(one_hot, axis=0) - one_hot) * one_hot, axis=1)
-    slot_index = expert_list * capacity + position_in
-    repeated = jnp.repeat(normed, top_count, axis=0)
-    outgoing = (
-        jnp.zeros((expert_count * capacity, width), jnp.bfloat16).at[slot_index].set(repeated)
-    )
-    arrived = lax.all_to_all(
-        outgoing.reshape(expert_count, capacity, width),
-        ("sp", "dp"),
-        split_axis=0,
-        concat_axis=0,
-        tiled=True,
-    )
+    slot_index = (expert_list * capacity + position_in).reshape(tok_count, top_count)
+    table = jnp.concatenate([slot_index.T.astype(jnp.float32), route_weights[0].T], axis=0)
+    arrived, tables = dispatch(normed, table, groups, sp_count, dp_count, capacity)
     flat_rows = arrived.reshape(-1, width)
     hidden = gated_rows(flat_rows, expert_gate[0], expert_up[0])
     finished = jnp.dot(hidden, expert_down[0], preferred_element_type=jnp.float32).astype(
         jnp.bfloat16
     )
-    received = lax.all_to_all(
-        finished.reshape(arrived.shape), ("sp", "dp"), split_axis=0, concat_axis=0, tiled=True
-    )
-    picked = received.reshape(expert_count * capacity, width)[slot_index]
-    picked = picked.reshape(tok_count, top_count, width).astype(jnp.float32)
-    routed = jnp.sum(picked * route_weights[0][:, :, None], axis=1)
-    result_rows = (mixed_rows + shared_out + routed).astype(jnp.bfloat16)
+    result_rows = combine(
+        finished.reshape(arrived.shape), tables, mixed_rows + shared_out, groups, sp_count, dp_count
+    )
     return result_rows[None]
+
+
+def places(groups, sp_count, dp_count):
+    row_count = sp_count // groups
+    sp_index = lax.axis_index("sp")
+    dp_index = lax.axis_index("dp")
+    layer = sp_index // row_count
+    seat = (sp_index % row_count) * dp_count + dp_index
+
+    def device_of(layer_to, seat_to):
+        return {"sp": layer_to * row_count + seat_to // dp_count, "dp": seat_to % dp_count}
+
+    return layer, seat, row_count * dp_count, device_of
+
+
+def greet(layer, seat, groups, seats, device_of):
+    barrier = pltpu.get_barrier_semaphore()
+    for j in range(1, groups):
+        pl.semaphore_signal(
+            barrier, inc=1, device_id=device_of((layer + j) % groups, seat),
+            device_id_type=pl.DeviceIdType.MESH,
+        )
+
+    @pl.loop(1, seats)
+    def _(i):
+        pl.semaphore_signal(
+            barrier, inc=1, device_id=device_of(layer, (seat + i) % seats),
+            device_id_type=pl.DeviceIdType.MESH,
+        )
+
+    pl.semaphore_wait(barrier, groups - 1 + seats - 1)
+
+
+def remote(src, dst, send_sem, recv_sem, device):
+    return pltpu.make_async_remote_copy(
+        src_ref=src, dst_ref=dst, send_sem=send_sem, recv_sem=recv_sem,
+        device_id=device, device_id_type=pl.DeviceIdType.MESH,
+    )
+
+
+def dispatch_kernel(
+    groups, sp_count, dp_count, capacity, rows_ref, table_ref, out_ref, tables_out,
+    all_rows, tables, picked, row_send, row_recv, table_send, table_recv, send, recv, own_sem,
+):
+    layer, seat, seats, device_of = places(groups, sp_count, dp_count)
+    tok_count, width = rows_ref.shape
+    top_count = table_ref.shape[0] // 2
+    slots = seats * capacity
+    step = min(512, width)
+    greet(layer, seat, groups, seats, device_of)
+
+    def row_copies(j):
+        source = (layer - j + groups) % groups
+        target = device_of((layer + j) % groups, seat)
+        return (
+            remote(table_ref, tables.at[layer], table_send.at[j], table_recv.at[j], target),
+            remote(rows_ref, all_rows.at[layer], row_send.at[j], row_recv.at[j], target),
+            remote(table_ref, tables.at[source], table_send.at[j], table_recv.at[j], target),
+            remote(rows_ref, all_rows.at[source], row_send.at[j], row_recv.at[j], target),
+        )
+
+    for j in range(1, groups):
+        for copy in row_copies(j)[:2]:
+            copy.start()
+    tables[layer] = table_ref[...]
+    slot_rows = lax.broadcasted_iota(jnp.int32, (slots, tok_count), 0) + layer * slots
+    slot_rows = slot_rows.astype(jnp.float32)
+
+    for j in range(groups):
+        source = (layer - j + groups) % groups
+        if j > 0:
+            for copy in row_copies(j)[2:]:
+                copy.wait_recv()
+        table = tables[source]
+        choose = jnp.zeros((slots, tok_count), jnp.float32)
+        for k in range(top_count):
+            choose = choose + jnp.where(slot_rows == table[k : k + 1, :], 1.0, 0.0)
+        choose = choose.astype(jnp.bfloat16)
+
+        @pl.loop(0, width // step)
+        def _(c):
+            columns = pl.ds(pl.multiple_of(c * step, step), step)
+            rows = rows_ref[:, columns] if j == 0 else all_rows[source, :, columns]
+            value = jnp.dot(choose, rows, preferred_element_type=jnp.float32)
+            for p in range(seats):
+                picked[j, p, :, columns] = value[p * capacity : (p + 1) * capacity].astype(
+                    jnp.bfloat16
+                )
+
+        @pl.loop(1, seats)
+        def _(i):
+            to = (seat + i) % seats
+            remote(
+                picked.at[j, to], out_ref.at[source, seat], send.at[j, i], recv.at[j, i],
+                device_of(layer, to),
+            ).start()
+
+        pltpu.make_async_copy(picked.at[j, seat], out_ref.at[source, seat], own_sem.at[j]).start()
+
+    tables_out[...] = tables[...]
+    for j in range(groups):
+        source = (layer - j + groups) % groups
+
+        @pl.loop(1, seats)
+        def _(i):
+            to = (seat + i) % seats
+            came = (seat - i + seats) % seats
+            remote(
+                picked.at[j, to], out_ref.at[source, came], send.at[j, i], recv.at[j, i],
+                device_of(layer, to),
+            ).wait()
+
+        pltpu.make_async_copy(picked.at[j, seat], out_ref.at[source, seat], own_sem.at[j]).wait()
+        if j > 0:
+            for copy in row_copies(j)[:2]:
+                copy.wait_send()
+
+
+def dispatch(rows, table, groups, sp_count, dp_count, capacity):
+    tok_count, width = rows.shape
+    seats = sp_count * dp_count // groups
+    vmem = pl.BlockSpec(memory_space=pltpu.VMEM)
+    return pl.pallas_call(
+        functools.partial(dispatch_kernel, groups, sp_count, dp_count, capacity),
+        out_shape=(
+            jax.ShapeDtypeStruct((groups, seats, capacity, width), jnp.bfloat16),
+            jax.ShapeDtypeStruct((groups,) + table.shape, jnp.float32),
+        ),
+        in_specs=[vmem, vmem],
+        out_specs=(pl.BlockSpec(memory_space=pl.ANY), vmem),
+        scratch_shapes=[
+            pltpu.VMEM((groups, tok_count, width), jnp.bfloat16),
+            pltpu.VMEM((groups,) + table.shape, jnp.float32),
+            pltpu.VMEM((groups, seats, capacity, width), jnp.bfloat16),
+            pltpu.SemaphoreType.DMA((groups,)),
+            pltpu.SemaphoreType.DMA((groups,)),
+            pltpu.SemaphoreType.DMA((groups,)),
+            pltpu.SemaphoreType.DMA((groups,)),
+            pltpu.SemaphoreType.DMA((groups, seats)),
+            pltpu.SemaphoreType.DMA((groups, seats)),
+            pltpu.SemaphoreType.DMA((groups,)),
+        ],
+        compiler_params=pltpu.CompilerParams(collective_id=0, has_side_effects=True),
+        name="dispatch",
+    )(rows, table)
+
+
+def combine_kernel(
+    groups, sp_count, dp_count, done_ref, tables, base_ref, out_ref,
+    back, partial, sums, send, recv, own_sem, sum_send, sum_recv,
+):
+    layer, seat, seats, device_of = places(groups, sp_count, dp_count)
+    tok_count, width = base_ref.shape
+    capacity = done_ref.shape[2]
+    top_count = tables.shape[1] // 2
+    slots = seats * capacity
+    step = min(512, width)
+    greet(layer, seat, groups, seats, device_of)
+    order = list(range(1, groups)) + [0]
+
+    def own_copy(j, source):
+        return pltpu.make_async_copy(
+            done_ref.at[source, seat], back.at[source, seat], own_sem.at[j]
+        )
+
+    for j in order:
+        source = (layer - j + groups) % groups
+
+        @pl.loop(1, seats)
+        def _(i):
+            to = (seat + i) % seats
+            remote(
+                done_ref.at[source, to], back.at[source, seat], send.at[j, i], recv.at[j, i],
+                device_of(layer, to),
+            ).start()
+
+        own_copy(j, source).start()
+
+    slot_rows = lax.broadcasted_iota(jnp.int32, (slots, tok_count), 0) + layer * slots
+    slot_rows = slot_rows.astype(jnp.float32)
+
+    for j in order:
+        source = (layer - j + groups) % groups
+
+        @pl.loop(1, seats)
+        def _(i):
+            to = (seat + i) % seats
+            came = (seat - i + seats) % seats
+            remote(
+                done_ref.at[source, to], back.at[source, came], send.at[j, i], recv.at[j, i],
+                device_of(layer, to),
+            ).wait()
+
+        own_copy(j, source).wait()
+        if j == 0:
+            for other in range(1, groups):
+                remote(
+                    partial.at[other], sums.at[other], sum_send.at[other], sum_recv.at[other],
+                    device_of((layer - other + groups) % groups, seat),
+                ).wait()
+        table = tables[source]
+        weigh = jnp.zeros((slots, tok_count), jnp.float32)
+        for k in range(top_count):
+            weigh = weigh + jnp.where(
+                slot_rows == table[k : k + 1, :], table[top_count + k : top_count + k + 1, :], 0.0
+            )
+        weigh = weigh.T
+        high = weigh.astype(jnp.bfloat16)
+        low = (weigh - high.astype(jnp.float32)).astype(jnp.bfloat16)
+
+        @pl.loop(0, width // step)
+        def _(c):
+            columns = pl.ds(pl.multiple_of(c * step, step), step)
+            rows = back[source, :, :, columns]
+            if capacity % 16:
+                rows = rows.astype(jnp.float32).reshape(slots, step).astype(jnp.bfloat16)
+            else:
+                rows = rows.reshape(slots, step)
+            value = jnp.dot(high, rows, preferred_element_type=jnp.float32) + jnp.dot(
+                low, rows, preferred_element_type=jnp.float32
+            )
+            if j == 0:
+                total = base_ref[:, columns] + value
+                for other in range(1, groups):
+                    total = total + sums[other, :, columns].astype(jnp.float32)
+                out_ref[:, columns] = total.astype(jnp.bfloat16)
+            else:
+                partial[j, :, columns] = value.astype(jnp.bfloat16)
+
+        if j > 0:
+            remote(
+                partial.at[j], sums.at[j], sum_send.at[j], sum_recv.at[j], device_of(source, seat)
+            ).start()
+
+
+def combine(finished, tables, base, groups, sp_count, dp_count):
+    tok_count, width = base.shape
+    seats = finished.shape[1]
+    vmem = pl.BlockSpec(memory_space=pltpu.VMEM)
+    return pl.pallas_call(
+        functools.partial(combine_kernel, groups, sp_count, dp_count),
+        out_shape=jax.ShapeDtypeStruct(base.shape, jnp.bfloat16),
+        in_specs=[pl.BlockSpec(memory_space=pl.ANY), vmem, vmem],
+        out_specs=vmem,
+        scratch_shapes=[
+            pltpu.VMEM(finished.shape, jnp.bfloat16),
+            pltpu.VMEM((groups, tok_count, width), jnp.bfloat16),
+            pltpu.VMEM((groups, tok_count, width), jnp.bfloat16),
+            pltpu.SemaphoreType.DMA((groups, seats)),
+            pltpu.SemaphoreType.DMA((groups, seats)),
+            pltpu.SemaphoreType.DMA((groups,)),
+            pltpu.SemaphoreType.DMA((groups,)),
+            pltpu.SemaphoreType.DMA((groups,)),
+        ],
+        compiler_params=pltpu.CompilerParams(collective_id=1, has_side_effects=True),
+        name="combine",
+    )(finished, tables, base)
 
 
 def solution(mesh):

time: 335 us -> 251 us (0.75); the launches traced: 329 us -> 249 us
  Pallas kernels: 0 us -> 140 us
  blocking collectives: 97.2 us -> 0 us
  waiting for transfers between devices: 113 us -> 20 us
  local copies, waits for them, and re-layouts: 42.5 us -> 20.3 us
  other arithmetic: 19.1 us -> 13.6 us
  starting transfers between devices: 22.9 us -> 18.1 us
  matrix products: 32.8 us -> 36.7 us
    pallas_call x0 -> x2, Pallas kernels: none -> 140 us  [the longest x1 76.7 us: combine(): pl.pallas_call(functools.partial(combine_kernel, groups, sp_count, dp_cou...]
    all_to_all x1 -> x0, blocking collectives: 97.2 us -> none  [shards(): lax.all_to_all(outgoing.reshape(expert_count, capacity, width), ('sp', 'd...]
    all_to_all x1 -> x0, waiting for transfers between devices: 91.9 us -> none  [shards(): lax.all_to_all(finished.reshape(arrived.shape), ('sp', 'dp'), split_axis=...]
    gather x1 -> x0, local copies, waits for them, and re-layouts: 7.96 us -> none  [shards(): picked = received.reshape(expert_count * capacity, width)[slot_index]]
    scatter x1 -> x0, local copies, waits for them, and re-layouts: 7.21 us -> none  [shards(): jnp.zeros((expert_count * capacity, width), jnp.bfloat16).at[slot_index]]
    reduce_sum x1 -> x0, other arithmetic: 6.33 us -> none  [shards(): routed = jnp.sum(picked * route_weights[0][:, :, None], axis=1)]
    convert_element_type x1 -> x0, local copies, waits for them, and re-layouts: 4.75 us -> none  [shards(): picked = picked.reshape(tok_count, top_count, width).astype(jnp.float32)]
    all_to_all x1 -> x0, starting transfers between devices: 4.05 us -> none  [shards(): lax.all_to_all(finished.reshape(arrived.shape), ('sp', 'dp'), split_axis=...]
  transfers between devices with their start and end apart: 5 -> 4, of which waited for: 5 -> 4; matrix products, arithmetic and copies ran while one was open for 5% -> 6% of each run, Pallas kernels for 0% -> 0%
where the time goes in v1:
time: 251 us; the launch traced here: 249 us
  Pallas kernels  140 us (56%)
  matrix products  36.7 us (15%)
  local copies, waits for them, and re-layouts  20.3 us (8%)
  waiting for transfers between devices  20 us (8%)
  starting transfers between devices  18.1 us (7%)
  other arithmetic  13.6 us (5%)
    pallas_call x1, Pallas kernels, combine(): pl.pallas_call(functools.partial(combine_kernel, groups, sp_count, dp_cou...  76.7 us
    pallas_call x1, Pallas kernels, dispatch(): pl.pallas_call(functools.partial(dispatch_kernel, groups, sp_count, dp_co...  63 us
    dot_general x1, matrix products, shards(): jnp.dot(hidden, expert_down[0], preferred_element_type=jnp.float32)  10.1 us
    unnamed x52, local copies, waits for them, and re-layouts  9.92 us
    unnamed x4, other arithmetic  8.97 us
    all_to_all x1, starting transfers between devices, shards(): lax.all_to_all(key_rows, 'sp', split_axis=2, concat_axis=1, tiled=True)  7.28 us
    all_to_all x1, waiting for transfers between devices, shards(): lax.all_to_all(attended, 'sp', split_axis=1, concat_axis=2, tiled=True)  7.17 us
    dot_general x2, matrix products, attend(): jnp.einsum('hqk,khd->qhd', weights, value_heads[:block_end], preferred_el...  6.65 us
  transfers between devices with their start and end apart: 4, of which 4 were waited for; matrix products, arithmetic and copies ran while one was open for 6% of the time, Pallas kernels for 0%

profile of v1, /device:TPU:0, one launch (start us, length us, event | category | flops | bytes accessed | tf_op | source)
XLA Modules:
  0.0 249.0 jit_solution(10550826647983603123)
XLA Ops:
  0.0 1.4 copy.56
  1.4 0.6 broadcast.89
  2.0 2.3 reduce.4
  4.3 0.8 reshape.116
  5.0 7.3 %all-to-all-start.1 = ((bf16[8,2,8192]{2,1,0:T(2,128)(2,1)}), bf16[8,2,8192]{2,1,0:T(2,128)(2,1)S(1)}, u32[]{:S(2)}, u32[]{:S(2)}) async-start(bf16[8,2,8192]{2,1,0:T(2,128)(2,1)} %reshape.116), calls=%async_computation.1 | async-start | bytes 524288 | tf_op jit(solution)/shard_map/all_to_all | solution.py:75
  12.7 2.2 reduce.2
  15.0 0.8 reshape.112
  15.8 5.5 %all-to-all-done.1 = bf16[8,2,8192]{2,1,0:T(2,128)(2,1)S(1)} async-done(((bf16[8,2,8192]{2,1,0:T(2,128)(2,1)}), bf16[8,2,8192]{2,1,0:T(2,128)(2,1)S(1)}, u32[]{:S(2)}, u32[]{:S(2)}) %all-to-all-start.1) | async-done | bytes 262176 | tf_op jit(solution)/shard_map/all_to_all | solution.py:75
  21.2 3.6 %all-to-all-start.2 = ((bf16[8,2,8192]{2,1,0:T(2,128)(2,1)}), bf16[8,2,8192]{2,1,0:T(2,128)(2,1)S(1)}, u32[]{:S(2)}, u32[]{:S(2)}) async-start(bf16[8,2,8192]{2,1,0:T(2,128)(2,1)} %reshape.112), calls=%async_computation.2 | async-start | bytes 524288 | tf_op jit(solution)/shard_map/all_to_all | solution.py:76
  25.5 2.2 reduce.3
  27.7 0.8 reshape.114
  28.5 1.2 reduce-window.6
  29.7 0.8 iota_compare_fusion.1
  30.4 3.0 %all-to-all-done.2 = bf16[8,2,8192]{2,1,0:T(2,128)(2,1)S(1)} async-done(((bf16[8,2,8192]{2,1,0:T(2,128)(2,1)}), bf16[8,2,8192]{2,1,0:T(2,128)(2,1)S(1)}, u32[]{:S(2)}, u32[]{:S(2)}) %all-to-all-start.2) | async-done | bytes 262176 | tf_op jit(solution)/shard_map/all_to_all | solution.py:76
  33.4 3.6 %all-to-all-start = ((bf16[8,2,8192]{2,1,0:T(2,128)(2,1)}), bf16[8,2,8192]{2,1,0:T(2,128)(2,1)S(1)}, u32[]{:S(2)}, u32[]{:S(2)}) async-start(bf16[8,2,8192]{2,1,0:T(2,128)(2,1)} %reshape.114), calls=%async_computation | async-start | bytes 524288 | tf_op jit(solution)/shard_map/all_to_all | solution.py:74
  37.0 0.6 fusion.50
  37.6 1.2 iota_compare_fusion
  39.1 0.7 slice.51
  40.2 0.7 slice.49
  41.1 4.4 %all-to-all-done = bf16[8,2,8192]{2,1,0:T(2,128)(2,1)S(1)} async-done(((bf16[8,2,8192]{2,1,0:T(2,128)(2,1)}), bf16[8,2,8192]{2,1,0:T(2,128)(2,1)S(1)}, u32[]{:S(2)}, u32[]{:S(2)}) %all-to-all-start) | async-done | bytes 262176 | tf_op jit(solution)/shard_map/all_to_all | solution.py:74
  45.9 0.7 fusion.49
  46.6 0.7 slice.38
  47.4 1.0 copy.61
  48.4 0.7 slice.45
  49.1 0.8 reshape_squeeze.8
  50.0 0.7 slice.40
  50.7 0.8 reshape_squeeze.9
  51.5 3.5 %fusion.51 = f32[2,512]{1,0:T(2,128)} fusion(f32[2,1024]{1,0:T(2,128)S(1)} %bitcast.142, f32[2,512]{1,0:T(2,128)} %get-tuple-element.12, pred[512,1024]{1,0:T(8,128)(4,1)S(1)} %copy-done.4, bf16[512,2,64]{0,2,1:T(8,128)(2,1)} %slice.45, bf16[1024,2,64]{0,2,1:T(8,128)(2,1)} %reshape_squeeze.8), kind=kOutput, calls=%fused_computation.70 | convolution fusion | flops 140510208 | bytes 933888 | tf_op jit(solution)/shard_map/sub | solution.py:40
  55.1 4.5 %fusion.17 = bf16[2,512,64]{1,2,0:T(8,128)(2,1)} fusion(bf16[1024,2,64]{0,2,1:T(8,128)(2,1)} %reshape_squeeze.9, f32[2,512]{1,0:T(2,128)} %fusion.51, f32[2,1024]{1,0:T(2,128)S(1)} %bitcast.143, f32[2,512]{1,0:T(2,128)} %get-tuple-element.12, pred[512,1024]{1,0:T(8,128)(4,1)S(1)} %copy-done.4, bf16[512,2,64]{0,2,1:T(8,128)(2,1)} %slice.45, ...), kind=kOutput, calls=%fused_computation.27 | convolution fusion | flops 275843072 | bytes 1327104 | tf_op jit(solution)/shard_map/hqk,khd->qhd/dot_general | solution.py:42
  59.5 1.0 copy.65
  60.8 2.0 fusion.52
  62.8 2.2 convolution_convert_fusion.1
  65.1 0.4 copy.80
  65.5 2.2 reduce.5
  67.8 0.8 reshape.118
  68.5 3.6 %all-to-all-start.3 = ((bf16[8,2,8192]{2,1,0:T(2,128)(2,1)}), bf16[8,2,8192]{2,1,0:T(2,128)(2,1)S(1)}, u32[]{:S(2)}, u32[]{:S(2)}) async-start(bf16[8,2,8192]{2,1,0:T(2,128)(2,1)} %reshape.118), calls=%async_computation.3 | async-start | bytes 524288 | tf_op jit(solution)/shard_map/all_to_all | solution.py:79
  72.8 0.6 pad_maximum_fusion.table_ref
  73.5 7.2 %all-to-all-done.3 = bf16[8,2,8192]{2,1,0:T(2,128)(2,1)S(1)} async-done(((bf16[8,2,8192]{2,1,0:T(2,128)(2,1)}), bf16[8,2,8192]{2,1,0:T(2,128)(2,1)S(1)}, u32[]{:S(2)}, u32[]{:S(2)}) %all-to-all-start.3) | async-done | bytes 262176 | tf_op jit(solution)/shard_map/all_to_all | solution.py:79
  81.2 3.1 %multiply_reduce_fusion.1 = (f32[128]{0:T(128)S(1)}, f32[128,2048]{1,0:T(8,128)S(1)}) fusion(bf16[128,1024]{0,1:T(8,128)(2,1)S(1)} %bitcast.137, bf16[1024,2048]{1,0:T(8,128)(2,1)} %param.21), kind=kOutput, calls=%fused_computation.31 | convolution fusion | flops 537395072 | bytes 5505536 | tf_op jit(solution)/shard_map/dot_general | solution.py:80
  84.6 0.4 multiply_convert_fusion.1.rows_ref
  85.1 0.8 copy-done.1
  85.9 0.5 fusion.53
  86.3 63.0 %dispatch.1 = (bf16[4,8,32,2048]{3,2,1,0:T(8,128)(2,1)}, f32[4,8,128]{2,1,0:T(8,128)}) custom-call(bf16[128,2048]{1,0:T(8,128)(2,1)} %copy-done.1, f32[8,128]{1,0:T(8,128)} %pad_maximum_fusion.table_ref), custom_call_target="tpu_custom_call" | custom-call | tf_op jit(solution)/shard_map/dispatch/pallas_call | solution.py:239
  149.3 6.6 %fusion.4 = f32[1024,512]{1,0:T(8,128)} fusion(bf16[1024,2048]{1,0:T(8,128)(2,1)} %bitcast.145, bf16[1,2048,512]{2,1,0:T(8,128)(2,1)} %param.27), kind=kOutput, calls=%fused_computation.9 | convolution fusion | flops 2147483648 | bytes 8388608 | tf_op jit(solution)/shard_map/dot_general | solution.py:51
  155.9 4.3 %convolution_add_fusion.base_ref = f32[128,2048]{1,0:T(8,128)} fusion(bf16[512,2048]{1,0:T(8,128)(2,1)} %param.31, bf16[128,2048]{1,0:T(8,128)(2,1)} %copy-done.1, bf16[2048,512]{1,0:T(8,128)(2,1)} %param.30, f32[128,512]{1,0:T(8,128)S(1)} %fusion.53, f32[128]{0:T(128)S(1)} %add_rsqrt_fusion.1, f32[128,2048]{1,0:T(8,128)S(1)} %get-tuple-element.14, ...), kind=kOutput, calls=%fused_computation.7 | convolution fusion | flops 538574848 | bytes 7610880 | tf_op jit(solution)/shard_map/dot_general | solution.py:91
  160.3 10.1 %convolution_convert_fusion = bf16[1024,2048]{1,0:T(8,128)(2,1)} fusion(bf16[1,512,2048]{2,1,0:T(8,128)(2,1)S(1)} %copy-done, f32[1024,512]{1,0:T(8,128)} %fusion.4, bf16[1024,2048]{1,0:T(8,128)(2,1)} %bitcast.146, bf16[1,2048,512]{2,1,0:T(8,128)(2,1)} %param.26), kind=kOutput, calls=%fused_computation.5 | convolution fusion | flops 4300210176 | bytes 14680064 | tf_op jit(solution)/shard_map/dot_general | solution.py:110
  170.4 76.7 %combine.1 = bf16[128,2048]{1,0:T(8,128)(2,1)} custom-call(bf16[4,8,32,2048]{3,2,1,0:T(8,128)(2,1)} %bitcast.122, f32[4,8,128]{2,1,0:T(8,128)} %get-tuple-element.8.tables, f32[128,2048]{1,0:T(8,128)} %convolution_add_fusion.base_ref), custom_call_target="tpu_custom_call" | custom-call | tf_op jit(solution)/shard_map/combine/pallas_call | solution.py:356
  247.1 1.9 copy.82
  (67 shorter events, 4.4 us)
Async XLA Ops:
  0.0 160.3 %copy-start = (bf16[1,512,2048]{2,1,0:T(8,128)(2,1)S(1)}, bf16[1,512,2048]{2,1,0:T(8,128)(2,1)}, u32[]{:S(2)}) copy-start(bf16[1,512,2048]{2,1,0:T(8,128)(2,1)} %param.28) | copy-start | bytes 6291460
  0.0 12.3 %copy-start.7 = (bf16[1,128,1024]{2,1,0:T(8,128)(2,1)S(1)}, bf16[1,128,1024]{2,1,0:T(8,128)(2,1)}, u32[]{:S(2)}) copy-start(bf16[1,128,1024]{2,1,0:T(8,128)(2,1)} %param.19) | copy-start | bytes 786436
  2.0 22.8 %copy-start.14 = (s32[1,128,4]{1,2,0:T(4,128)S(1)}, s32[1,128,4]{1,2,0:T(4,128)}, u32[]{:S(2)}) copy-start(s32[1,128,4]{1,2,0:T(4,128)} %param.24) | copy-start | bytes 6148
  4.3 20.8 %copy-start.8 = (bf16[1,128,1024]{2,1,0:T(8,128)(2,1)S(1)}, bf16[1,128,1024]{2,1,0:T(8,128)(2,1)}, u32[]{:S(2)}) copy-start(bf16[1,128,1024]{2,1,0:T(8,128)(2,1)} %param.17) | copy-start | bytes 786436
  5.0 16.2 %all-to-all-start.1 = ((bf16[8,2,8192]{2,1,0:T(2,128)(2,1)}), bf16[8,2,8192]{2,1,0:T(2,128)(2,1)S(1)}, u32[]{:S(2)}, u32[]{:S(2)}) async-start(bf16[8,2,8192]{2,1,0:T(2,128)(2,1)} %reshape.116), calls=%async_computation.1 | async-start | bytes 524288 | tf_op jit(solution)/shard_map/all_to_all | solution.py:75
  15.0 22.0 %copy-start.15 = (f32[1,2,1024]{2,1,0:T(2,128)S(1)}, f32[1,2,1024]{2,1,0:T(2,128)}, u32[]{:S(2)}) copy-start(f32[1,2,1024]{2,1,0:T(2,128)} %param.20) | copy-start | bytes 24580
  21.2 12.2 %all-to-all-start.2 = ((bf16[8,2,8192]{2,1,0:T(2,128)(2,1)}), bf16[8,2,8192]{2,1,0:T(2,128)(2,1)S(1)}, u32[]{:S(2)}, u32[]{:S(2)}) async-start(bf16[8,2,8192]{2,1,0:T(2,128)(2,1)} %reshape.112), calls=%async_computation.2 | async-start | bytes 524288 | tf_op jit(solution)/shard_map/all_to_all | solution.py:76
  33.4 12.1 %all-to-all-start = ((bf16[8,2,8192]{2,1,0:T(2,128)(2,1)}), bf16[8,2,8192]{2,1,0:T(2,128)(2,1)S(1)}, u32[]{:S(2)}, u32[]{:S(2)}) async-start(bf16[8,2,8192]{2,1,0:T(2,128)(2,1)} %reshape.114), calls=%async_computation | async-start | bytes 524288 | tf_op jit(solution)/shard_map/all_to_all | solution.py:74
  45.8 4.1 %copy-start.6 = (bf16[1,4,128,128]{2,3,1,0:T(8,128)(2,1)S(1)}, bf16[1,4,128,128]{2,3,1,0:T(8,128)(2,1)}, u32[]{:S(2)}) copy-start(bf16[1,4,128,128]{2,3,1,0:T(8,128)(2,1)} %slice.51) | copy-start | bytes 393220
  45.8 5.7 %copy-start.4 = (pred[512,1024]{1,0:T(8,128)(4,1)S(1)}, pred[512,1024]{1,0:T(8,128)(4,1)}, u32[]{:S(2)}) copy-start(pred[512,1024]{1,0:T(8,128)(4,1)} %iota_compare_fusion) | copy-start | bytes 1572868
  51.5 3.6 %copy-start.10 = (bf16[1024,2,64]{0,2,1:T(8,128)(2,1)S(1)}, bf16[1024,2,64]{0,2,1:T(8,128)(2,1)}, u32[]{:S(2)}) copy-start(bf16[1024,2,64]{0,2,1:T(8,128)(2,1)} %reshape_squeeze.8) | copy-start | bytes 786436
  55.1 5.5 %copy-start.5 = (bf16[1,4,128,128]{2,3,1,0:T(8,128)(2,1)S(1)}, bf16[1,4,128,128]{2,3,1,0:T(8,128)(2,1)}, u32[]{:S(2)}) copy-start(bf16[1,4,128,128]{2,3,1,0:T(8,128)(2,1)} %slice.49) | copy-start | bytes 393220
  55.1 5.7 %copy-start.9 = (pred[512,512]{0,1:T(8,128)(4,1)S(1)}, pred[512,512]{0,1:T(8,128)(4,1)}, u32[]{:S(2)}) copy-start(pred[512,512]{0,1:T(8,128)(4,1)} %iota_compare_fusion.1) | copy-start | bytes 786436
  55.1 5.7 %copy-start.11 = (bf16[512,2,64]{0,2,1:T(8,128)(2,1)S(1)}, bf16[512,2,64]{0,2,1:T(8,128)(2,1)}, u32[]{:S(2)}) copy-start(bf16[512,2,64]{0,2,1:T(8,128)(2,1)} %slice.38) | copy-start | bytes 393220
  64.9 7.9 %copy-start.16 = (f32[1,128,4]{1,2,0:T(4,128)S(1)}, f32[1,128,4]{1,2,0:T(4,128)}, u32[]{:S(2)}) copy-start(f32[1,128,4]{1,2,0:T(4,128)} %param.25) | copy-start | bytes 6148
  68.5 12.1 %all-to-all-start.3 = ((bf16[8,2,8192]{2,1,0:T(2,128)(2,1)}), bf16[8,2,8192]{2,1,0:T(2,128)(2,1)S(1)}, u32[]{:S(2)}, u32[]{:S(2)}) async-start(bf16[8,2,8192]{2,1,0:T(2,128)(2,1)} %reshape.118), calls=%async_computation.3 | async-start | bytes 524288 | tf_op jit(solution)/shard_map/all_to_all | solution.py:79
  81.1 3.1 %copy-start.2 = (bf16[1,128,2048]{2,1,0:T(8,128)(2,1)S(1)}, bf16[1,128,2048]{2,1,0:T(8,128)(2,1)}, u32[]{:S(2)}) copy-start(bf16[1,128,2048]{2,1,0:T(8,128)(2,1)} %param.16) | copy-start | bytes 1572868
  81.1 3.1 %copy-start.12 = (f32[2048]{0:T(1024)S(1)}, f32[2048]{0:T(1024)}, u32[]{:S(2)}) copy-start(f32[2048]{0:T(1024)} %param.22) | copy-start | bytes 24580
  81.2 3.5 %copy-start.13 = (f32[2048]{0:T(1024)S(1)}, f32[2048]{0:T(1024)}, u32[]{:S(2)}) copy-start(f32[2048]{0:T(1024)} %param.23) | copy-start | bytes 24580
  84.2 1.6 copy-start.3
  85.1 0.8 copy-start.1
